TPU v7x, 32 devices: a whole 2x2x4 slice. The times are simulated.
32 devices in a mesh: fs: 8 (over z, y), tp: 4 (over x, core).
Axes of the slice: x: 2, y: 2, z: 4, core: 2. Of those that a mesh axis runs over, the one named last changes fastest.
Arguments:
- resid: bfloat16 [8192, 2048], P(('fs', 'tp')), may hold values from -6 to 6
- mix_gain: float32 [2048], replicated, may hold values from 0.1 to 1.9
- w_query: bfloat16 [2048, 1024], P('fs', 'tp'), may hold values from -0.125 to 0.125
- w_key: bfloat16 [2048, 1024], P('fs', 'tp'), may hold values from -0.125 to 0.125
- w_value: bfloat16 [2048, 2048], P('fs', 'tp'), may hold values from -0.125 to 0.125
- w_gate: bfloat16 [2048, 2048], P('fs', 'tp'), may hold values from -0.125 to 0.125
- w_output: bfloat16 [2048, 2048], P('tp', 'fs'), may hold values from -0.125 to 0.125
- decay_rate: float32 [8], P('tp'), may hold values from 0.0008 to 0.034, as said below
- mlp_gain: float32 [2048], replicated, may hold values from 0.1 to 1.9
- w_up: bfloat16 [2048, 8192], P('fs', 'tp'), may hold values from -0.125 to 0.125
- w_down: bfloat16 [8192, 2048], P('tp', 'fs'), may hold values from -0.0625 to 0.0625
Outputs:
- layer_out: bfloat16 [8192, 2048], P(('fs', 'tp'))
Inputs may be any that keep to these rules, and one draw needn't show every extreme that they name: `decay_rate`: decay rates per position, one for each head.
All inputs are finite; a program needn't handle non-finite values.
Results may differ from a plain program's by a relative error of at most 0.038.
Values may be sent and summed in bfloat16 or wider, within the bound.
A program may use at most 64 MiB of HBM per device.

v0:
```python
import functools

import jax
import jax.numpy as jnp
from jax import lax
from jax.experimental import pallas as pl
from jax.experimental.pallas import tpu as pltpu
from jax.sharding import PartitionSpec as P

DK = 128
DV = 256
LENGTH = 512
MESH = pl.DeviceIdType.MESH
EPS = 1e-06
F32 = jnp.float32
BF16 = jnp.bfloat16


def tile_of(width):
    return 256 if width % 256 == 0 else 128


def kernel(fs, tp, resid_ref, mix_gain_ref, mlp_gain_ref, rate_ref, w1_ref, w2_ref, w3_ref, w4_ref, wo_ref, wu_ref, wd_ref,
           out_ref, wq, wo, wu, wd, xn, xn2, proj, gated, hidden, part1, core1, chip1, part2, chip2,
           after, ring_send, ring_recv, own_sem, in_sem, ag_send, ag_recv, line_send, line_recv,
           swap_send, swap_recv, core1_send, core1_recv, chip1_send, chip1_recv, all_send, all_recv,
           core2_send, core2_recv, chip2_send, chip2_recv):
    half = fs // 2
    lines = fs // 2
    in_refs = (w1_ref, w2_ref, w3_ref, w4_ref)
    deep_q = w1_ref.shape[0]
    chips = tp // 2
    rows = resid_ref.shape[0]
    heads = rate_ref.shape[0]
    tokens = rows * tp
    me_f = lax.axis_index("fs")
    me_t = lax.axis_index("tp")
    pair = me_f % 2
    line = me_f // 2
    other_f = 2 * line + 1 - pair
    chip = me_t // 2
    core = me_t % 2
    other_t = 2 * chip + 1 - core

    def place(i):
        col = i % 2
        at = i // 2
        return at * (1 - col) + (fs - 1 - at) * col

    def index(p):
        col = p // half
        return 2 * (p * (1 - col) + (fs - 1 - p) * col) + col

    my_place = place(me_f)
    target = (index((my_place + 1) % fs), index((my_place + fs - 1) % fs))

    def owner(way, dist):
        if way == 0:
            return index((my_place + fs - dist) % fs)
        return index((my_place + dist) % fs)

    def peer(d):
        return (me_t + d) % tp

    def beside(e):
        return 2 * ((chip + e) % chips) + core

    def step_to(way):
        return me_f + 2 if way == 0 else me_f - 2

    def line_has(way, dist):
        return line >= dist if way == 0 else line + dist <= lines - 1

    def line_next(way):
        return line_has(1 - way, 1)

    first_row = pl.multiple_of(me_f * deep_q, deep_q)
    loads = []
    left = 0
    for n, ref in enumerate(in_refs):
        copy = pltpu.make_async_copy(
            ref, wq.at[pl.ds(first_row, deep_q), left:left + ref.shape[1]], in_sem.at[n])
        copy.start()
        loads.append(copy)
        left += ref.shape[1]

    barrier = pltpu.get_barrier_semaphore()

    def greet(where):
        pl.semaphore_signal(barrier, inc=1, device_id=where, device_id_type=MESH)

    for way in range(2):
        greet((target[way], me_t))
    for d in range(1, tp):
        greet((me_f, peer(d)))
        if d % 2 == 0:
            greet((other_f, peer(d)))
    greet((other_f, me_t))
    for way in range(2):
        at = (line + (1 if way == 0 else lines - 1)) % lines
        greet((2 * at + pair, me_t))
    pl.semaphore_wait(barrier, 2 + (tp - 1) + (chips - 1) + 1 + 2)

    groups = ((None, wq, False), (wo_ref, wo, True))
    started = []

    def go(copy, on=None):
        if on is None:
            copy.start()
        else:
            @pl.when(on)
            def _():
                copy.start()
        started.append((copy, on))

    def remote(src, dst, s_sem, r_sem, where):
        return pltpu.make_async_remote_copy(
            src_ref=src, dst_ref=dst, send_sem=s_sem, recv_sem=r_sem, device_id=where,
            device_id_type=MESH)

    def landed(dst, s_sem, r_sem):
        return remote(dst, dst, s_sem, r_sem, (me_f, other_t))

    def span(at, size):
        return pl.ds(pl.multiple_of(at, size), size)

    def slot(w, who, h):
        source, whole, slotted = groups[w]
        hr = (deep_q if w == 0 else source.shape[0]) // 2
        deep = 2 * hr
        if slotted:
            return whole.at[who, pl.ds(h * hr, hr), :]
        return whole.at[pl.ds(pl.multiple_of(who * deep + h * hr, hr), hr), :]

    rounds = []
    for w in range(2):
        for dist in range(1, half):
            rounds += [(w, dist, 0), (w, dist, 1)]
        rounds.append((w, half, 0))
    per = fs - 1

    def half_of(way, turn):
        return turn if way == 0 else 1 - turn

    def send(k):
        w, dist, turn = rounds[k]
        for way in range(2):
            h = half_of(way, turn)
            who = owner(way, dist - 1)
            src = slot(w, who, h)
            if dist == 1 and w == 1:
                hr = wo_ref.shape[0] // 2
                src = wo_ref.at[pl.ds(h * hr, hr), :]
            go(remote(src, slot(w, who, h), ring_send.at[way, k], ring_recv.at[way, k],
                      (target[way], me_t)))

    def arrive(k):
        w, dist, turn = rounds[k]
        for way in range(2):
            here = slot(w, owner(way, dist), half_of(way, turn))
            landed(here, ring_send.at[way, k], ring_recv.at[way, k]).wait_recv()
        if dist + 1 < half or (dist + 1 == half and turn == 0):
            send(k + 2)

    up_cols = wu.shape[1]
    deep = wu_ref.shape[0]
    down_rows = wd.shape[1]

    def piece(g, who):
        return wu.at[span(who * deep, deep), :] if g == 0 else wd.at[who]

    def share(g, y):
        if g == 0:
            return wu_ref.at[:, span(y * up_cols, up_cols)]
        return wd_ref.at[span(y * down_rows, down_rows), :]

    def swap_start(g):
        go(remote(share(g, 1 - pair), piece(g, me_f), swap_send.at[g], swap_recv.at[g],
                  (other_f, me_t)))

    def swap_wait(g):
        landed(piece(g, other_f), swap_send.at[g], swap_recv.at[g]).wait_recv()

    line_rounds = [(g, dist, turn) for g in range(2) for dist in range(1, lines) for turn in range(2)]
    per_line = 2 * (lines - 1)

    def line_owner(way, dist, turn):
        at = line - dist if way == 0 else line + dist
        return 2 * at + (pair if turn == 0 else 1 - pair)

    def line_send_round(m, ways=(0, 1)):
        g, dist, turn = line_rounds[m]
        for way in ways:
            who = line_owner(way, dist - 1, turn)
            src = share(g, pair) if dist == 1 and turn == 0 else piece(g, who)
            on = line_next(way) if dist == 1 else jnp.logical_and(line_next(way), line_has(way, dist - 1))
            go(remote(src, piece(g, who), line_send.at[way, m], line_recv.at[way, m],
                      (step_to(way), me_t)), on)

    def line_arrive(m):
        g, dist, turn = line_rounds[m]
        for way in range(2):
            copy = landed(piece(g, line_owner(way, dist, turn)), line_send.at[way, m],
                          line_recv.at[way, m])

            @pl.when(line_has(way, dist))
            def _():
                copy.wait_recv()
            if dist + 1 < lines:
                line_send_round(m + 2, (way,))

    for copy in loads:
        copy.wait()
    send(0)
    send(1)
    own = [None]
    for n, (src, dst) in enumerate((
            (wo_ref, wo.at[me_f]),
            (share(0, pair), piece(0, me_f)),
            (share(1, pair), piece(1, me_f)))):
        copy = pltpu.make_async_copy(src, dst, own_sem.at[n])
        own.append(copy)

    my_rows = span(me_t * rows, rows)

    def norm(source, gain_ref):
        wide = source.astype(F32)
        mean = jnp.mean(wide * wide, axis=-1, keepdims=True)
        return (wide * lax.rsqrt(mean + EPS) * gain_ref[...]).astype(BF16)

    step = 64

    def norm_into(buf, first, source_ref, gain_ref):
        @pl.loop(0, rows // step)
        def _(i):
            at = pl.multiple_of(i * step, step)
            buf[pl.ds(pl.multiple_of(first + at, step), step), :] = norm(
                source_ref[pl.ds(at, step), :], gain_ref)

    def ag_block(t):
        return xn.at[span(t * rows, rows), :]

    ag_copies = [remote(ag_block(me_t), ag_block(me_t), ag_send.at[d - 1], ag_recv.at[d - 1],
                        (me_f, peer(d))) for d in range(1, tp)]

    def ag_start():
        for copy in ag_copies:
            copy.start()

    def ag_wait():
        for d in range(1, tp):
            landed(ag_block(peer(tp - d)), ag_send.at[d - 1], ag_recv.at[d - 1]).wait_recv()

    def project():
        width = proj.shape[1]
        t = tile_of(width)

        @pl.loop(0, width // t)
        def _(j):
            cols = pl.ds(pl.multiple_of(j * t, t), t)
            proj[:, cols] = jnp.dot(xn[...], wq[:, cols], preferred_element_type=F32).astype(BF16)

    def retain():
        kq = heads * DK
        vq = heads * DV
        count = tokens // LENGTH
        for head in range(heads):
            rate = rate_ref[head]

            @pl.loop(0, count)
            def _(n):
                base = pl.multiple_of(n * LENGTH, LENGTH)
                rs = pl.ds(base, LENGTH)
                q = proj[rs, head * DK:(head + 1) * DK]
                k = proj[rs, kq + head * DK:kq + (head + 1) * DK]
                v = proj[rs, 2 * kq + head * DV:2 * kq + (head + 1) * DV]
                g = proj[rs, 2 * kq + vq + head * DV:2 * kq + vq + (head + 1) * DV].astype(F32)
                scores = lax.dot_general(q, k, (((1,), (1,)), ((), ())), preferred_element_type=F32)
                t_at = lax.broadcasted_iota(jnp.int32, (LENGTH, LENGTH), 0)
                s_at = lax.broadcasted_iota(jnp.int32, (LENGTH, LENGTH), 1)
                gap = t_at - s_at
                decay = jnp.exp(-rate * jnp.maximum(gap, 0).astype(F32)) * (DK ** -0.5)
                scores = jnp.where(gap >= 0, scores * decay, 0.0).astype(BF16)
                mixed = jnp.dot(scores, v, preferred_element_type=F32)
                mean = jnp.mean(mixed, axis=-1, keepdims=True)
                off = mixed - mean
                var = jnp.mean(off * off, axis=-1, keepdims=True)
                grouped = off * lax.rsqrt(var + EPS)
                gated[rs, head * DV:(head + 1) * DV] = (g / (1.0 + jnp.exp(-g)) * grouped).astype(BF16)

    def mix_block(x, c):
        return part1.at[span((2 * x + c) * rows, rows), :]

    def mix_out():
        cols = wo.shape[2]

        @pl.loop(0, fs)
        def _(j):
            part1[:, span(j * cols, cols)] = jnp.dot(
                gated[...], wo[j], preferred_element_type=F32).astype(BF16)
        order = [e % chips for e in range(1, chips + 1)]
        for e in order:
            x = (chip + e) % chips
            go(remote(mix_block(x, 1 - core), core1.at[e], core1_send.at[e], core1_recv.at[e],
                      (me_f, other_t)))
        for e in order:
            landed(core1.at[e], core1_send.at[e], core1_recv.at[e]).wait_recv()
            if e:
                first = beside(e) * rows

                @pl.loop(0, rows // step)
                def _(i):
                    at = pl.ds(pl.multiple_of(first + i * step, step), step)
                    more = core1[e, span(i * step, step), :].astype(F32)
                    part1[at, :] = (part1[at, :].astype(F32) + more).astype(BF16)
                go(remote(ag_mix(beside(e)), chip1.at[e - 1], chip1_send.at[e - 1],
                          chip1_recv.at[e - 1], (me_f, beside(e))))

    def ag_mix(t):
        return part1.at[span(t * rows, rows), :]

    def mix_end():
        for e in range(1, chips):
            landed(chip1.at[e - 1], chip1_send.at[e - 1], chip1_recv.at[e - 1]).wait_recv()

        @pl.loop(0, rows // step)
        def _(i):
            at = span(i * step, step)
            total = part1[pl.ds(pl.multiple_of(me_t * rows + i * step, step), step), :].astype(F32)
            total = total + core1[0, at, :].astype(F32)
            for e in range(1, chips):
                total = total + chip1[e - 1, at, :].astype(F32)
            sum_ = (resid_ref[at, :].astype(F32) + total).astype(BF16)
            after[at, :] = sum_
            xn2[pl.ds(pl.multiple_of(block(pair, me_t) * rows + i * step, step), step), :] = norm(
                sum_, mlp_gain_ref)

    def block(y, t):
        return (t % 2) * (2 * chips) + y * chips + t // 2

    def wide(y, t, part=None):
        first = block(y, t) * rows
        hr = rows // 2
        if part is None:
            return xn2.at[span(first, rows), :]
        return xn2.at[pl.ds(pl.multiple_of(first + part * hr, hr), hr), :]

    more_chips = chips - 1
    pieces = 1 + 3 * more_chips

    def all_copy(n, ref, where):
        go(remote(ref, ref, all_send.at[n], all_recv.at[n], where))

    def all_landed(n, ref):
        landed(ref, all_send.at[n], all_recv.at[n]).wait_recv()

    def across(n, ref):
        all_copy(pieces + n, ref, (me_f, other_t))

    def all_first():
        ref = wide(pair, me_t)
        all_copy(0, ref, (other_f, me_t))
        for e in range(1, chips):
            all_copy(e, ref, (me_f, beside(e)))
        all_copy(2 * pieces, ref, (me_f, other_t))

    def all_second():
        ref = wide(1 - pair, me_t)
        all_landed(0, ref)
        for e in range(1, chips):
            all_copy(more_chips + e, wide(1 - pair, me_t, 0), (me_f, beside(e)))
        across(0, ref)
        for e in range(1, chips):
            t = beside(chips - e)
            all_landed(e, wide(pair, t))
            all_copy(2 * more_chips + e, wide(pair, t, 1), (other_f, me_t))
            across(e, wide(pair, t))

    def all_third():
        for part in range(2):
            for e in range(1, chips):
                n = (1 + part) * more_chips + e
                ref = wide(1 - pair, beside(chips - e), part)
                all_landed(n, ref)
                across(n, ref)
        all_landed(2 * pieces, wide(pair, other_t))
        all_landed(pieces, wide(1 - pair, other_t))
        for e in range(1, chips):
            t = 2 * ((chip + chips - e) % chips) + 1 - core
            all_landed(pieces + e, wide(pair, t))
            for part in range(2):
                all_landed(pieces + (1 + part) * more_chips + e, wide(1 - pair, t, part))

    def lift():
        t = tile_of(up_cols)

        @pl.loop(0, 2)
        def _(i):
            at = span(i * tokens, tokens)

            @pl.loop(0, up_cols // t)
            def _(j):
                cols = span(j * t, t)
                up = jnp.maximum(jnp.dot(xn2[at, :], wu[:, cols], preferred_element_type=F32), 0.0)
                hidden[at, cols] = (up * up).astype(BF16)

    cw = wd.shape[2]
    r2 = 2 * chips - 1

    def mlp_copies(who):
        cols = span(who * cw, cw)
        first = core * tokens
        side = remote(part2.at[span((1 - core) * tokens, tokens), cols], xn.at[:, cols],
                      core2_send.at[who], core2_recv.at[who], (me_f, other_t))
        side_in = landed(xn.at[:, cols], core2_send.at[who], core2_recv.at[who])
        outs, ins = [], []
        n = 0
        for dy in range(2):
            for e in range(chips):
                if dy == 0 and e == 0:
                    continue
                y = pair if dy == 0 else 1 - pair
                t = beside(e)
                dst = chip2.at[n, :, cols]
                outs.append(remote(part2.at[span(block(y, t) * rows, rows), cols], dst,
                                   chip2_send.at[n, who], chip2_recv.at[n, who],
                                   (me_f if dy == 0 else other_f, t)))
                ins.append(landed(dst, chip2_send.at[n, who], chip2_recv.at[n, who]))
                n += 1
        return side, side_in, outs, ins

    finals = []

    def lower(who, on=None):
        side, side_in, outs, ins = mlp_copies(who)
        cols = span(who * cw, cw)
        mine = block(pair, me_t) * rows

        def run():
            @pl.loop(0, 2)
            def _(i):
                at = span(((1 - core) * (1 - i) + core * i) * tokens, tokens)
                part2[at, cols] = jnp.dot(
                    hidden[at, :], wd[who], preferred_element_type=F32).astype(BF16)

                @pl.when(i == 0)
                def _():
                    side.start()
            side_in.wait_recv()

            @pl.loop(0, tokens // 128)
            def _(i):
                at = pl.ds(pl.multiple_of(core * tokens + i * 128, 128), 128)
                more = xn[span(i * 128, 128), cols].astype(F32)
                part2[at, cols] = (part2[at, cols].astype(F32) + more).astype(BF16)
            for copy in outs:
                copy.start()

        def end():
            for copy in ins:
                copy.wait_recv()
            total = part2[span(mine, rows), cols].astype(F32)
            for n in range(r2):
                total = total + chip2[n, :, cols].astype(F32)
            out_ref[:, cols] = (after[:, cols].astype(F32) + total).astype(BF16)
            side.wait_send()
            for copy in outs:
                copy.wait_send()

        if on is None:
            run()
        else:
            pl.when(on)(run)
        finals.append((end, on))

    norm_into(xn, me_t * rows, resid_ref, mix_gain_ref)
    ag_start()
    for copy in own[1:]:
        copy.start()

    own_at = {per - 3: [per], per - 2: [per + 1]}

    for k in range(2 * per):
        arrive(k)
        for extra in own_at.get(k, ()):
            send(extra)
        if k == per - 1:
            line_send_round(0)
            ag_wait()
            project()
        elif k == per:
            swap_start(0)
        elif k == per + 1:
            retain()
        elif k == 2 * per - 2:
            swap_wait(0)
            line_send_round(1)
            swap_start(1)
        elif k == 2 * per - 1:
            own[1].wait()
            mix_out()

    last_d = per_line - 2
    for m in range(2 * per_line):
        line_arrive(m)
        if m == last_d - 1:
            line_send_round(per_line)
        elif m == last_d:
            swap_wait(1)
            line_send_round(per_line + 1)
        if m == per_line + (-3):
            for copy in ag_copies:
                copy.wait_send()
            mix_end()
            all_first()
        elif m == per_line + (-1):
            all_second()
        elif m == per_line:
            own[2].wait()
            own[3].wait()
            all_third()
            lift()
            lower(me_f)
            lower(other_f)
        if m >= per_line:
            _, dist, turn = line_rounds[m]
            for way in range(2):
                lower(line_owner(way, dist, turn), line_has(way, dist))

    for end, on in finals:
        if on is None:
            end()
        else:
            pl.when(on)(end)
    for copy, on in started:
        if on is None:
            copy.wait_send()
        else:
            pl.when(on)(copy.wait_send)


def on_device(fs, tp, resid, mix_gain, w_query, w_key, w_value, w_gate, w_output, decay_rate,
              mlp_gain, w_up, w_down):
    rows, width = resid.shape
    tokens = rows * tp
    in_width = w_query.shape[1] + w_key.shape[1] + w_value.shape[1] + w_gate.shape[1]
    chips = tp // 2
    wide = 2 * (1 + 3 * (chips - 1)) + 1
    vmem = pl.BlockSpec(memory_space=pltpu.VMEM)
    hbm = pl.BlockSpec(memory_space=pl.ANY)
    dma = pltpu.SemaphoreType.DMA
    cols = width // fs
    return pl.pallas_call(
        functools.partial(kernel, fs, tp),
        out_shape=jax.ShapeDtypeStruct((rows, width), BF16),
        in_specs=[vmem] * 3 + [pl.BlockSpec(memory_space=pltpu.SMEM)] + [hbm] * 7,
        out_specs=vmem,
        scratch_shapes=[
            pltpu.VMEM((width, in_width), BF16),
            pltpu.VMEM((fs, w_output.shape[0], cols), BF16),
            pltpu.VMEM((width, w_up.shape[1] // 2), BF16),
            pltpu.VMEM((fs, w_down.shape[0] // 2, cols), BF16),
            pltpu.VMEM((tokens, width), BF16),
            pltpu.VMEM((2 * tokens, width), BF16),
            pltpu.VMEM((tokens, in_width), BF16),
            pltpu.VMEM((tokens, w_output.shape[0]), BF16),
            pltpu.VMEM((2 * tokens, w_up.shape[1] // 2), BF16),
            pltpu.VMEM((tokens, width), BF16),
            pltpu.VMEM((chips, rows, width), BF16),
            pltpu.VMEM((chips - 1, rows, width), BF16),
            pltpu.VMEM((2 * tokens, width), BF16),
            pltpu.VMEM((2 * chips - 1, rows, width), BF16),
            pltpu.VMEM((rows, width), BF16),
            dma((2, 2 * (fs - 1))),
            dma((2, 2 * (fs - 1))),
            dma((3,)),
            dma((4,)),
            dma((tp - 1,)),
            dma((tp - 1,)),
            dma((2, 2 * (fs - 2))),
            dma((2, 2 * (fs - 2))),
            dma((2,)),
            dma((2,)),
            dma((chips,)),
            dma((chips,)),
            dma((chips - 1,)),
            dma((chips - 1,)),
            dma((wide,)),
            dma((wide,)),
            dma((fs,)),
            dma((fs,)),
            dma((2 * chips - 1, fs)),
            dma((2 * chips - 1, fs)),
        ],
        compiler_params=pltpu.CompilerParams(
            collective_id=0, has_side_effects=True, vmem_limit_bytes=67043328),
    )(resid, mix_gain[None, :], mlp_gain[None, :], decay_rate, w_query, w_key, w_value,
      w_gate, w_output, w_up, w_down)


def solution(mesh):
    placed = (
        P(("fs", "tp"), None),
        P(),
        P("fs", "tp"),
        P("fs", "tp"),
        P("fs", "tp"),
        P("fs", "tp"),
        P("tp", "fs"),
        P("tp"),
        P(),
        P("fs", "tp"),
        P("tp", "fs"),
    )
    sizes = dict(mesh.shape)
    return jax.shard_map(
        functools.partial(on_device, sizes["fs"], sizes["tp"]), mesh=mesh, in_specs=placed,
        out_specs=P(("fs", "tp"), None), check_vma=False)
```

profile of v0, /device:TPU:0, one launch (start us, length us, event | category | flops | bytes accessed | tf_op | source)
XLA Modules:
  0.0 242.9 jit_solution(6895588465565285535)
XLA Ops:
  0.0 240.6 %shard_map.109 = bf16[256,2048]{1,0:T(8,128)(2,1)} custom-call(bf16[256,2048]{1,0:T(8,128)(2,1)} %resid_ref.1, f32[1,2048]{1,0:T(1,128)} %bitcast.2, f32[1,2048]{1,0:T(1,128)} %bitcast.3, f32[2]{0:T(128)} %rate_ref.1, bf16[256,256]{1,0:T(8,128)(2,1)} %w1_ref.1, bf16[256,256]{1,0:T(8,128)(2,1)} %w2_ref.1, bf16[256,512]{1,0:T(8,128)(2,1)} %w3_ref.1, ...), custom_call_target="tpu_custom_call" | custom-call | tf_op jit(solution)/shard_map/pallas_call | solution.py:553
  240.6 2.3 copy.13
where the time goes:
time: 243 us
  Pallas kernels  241 us (99%)
    pallas_call x1, Pallas kernels, on_device(): pl.pallas_call(functools.partial(kernel, fs, tp), out_shape=jax.ShapeDtyp...  241 us

commit v1 on v0

v1 whole, which is shorter than its diff:
```python
import functools

import jax
import jax.numpy as jnp
from jax import lax
from jax.experimental import pallas as pl
from jax.experimental.pallas import tpu as pltpu
from jax.sharding import PartitionSpec as P

DK = 128
DV = 256
LENGTH = 512
MESH = pl.DeviceIdType.MESH
EPS = 1e-06
F32 = jnp.float32
BF16 = jnp.bfloat16


def tile_of(width):
    return 256 if width % 256 == 0 else 128


def kernel(fs, tp, resid_ref, mix_gain_ref, mlp_gain_ref, rate_ref, w1_ref, w2_ref, w3_ref, w4_ref, wo_ref, wu_ref, wd_ref,
           out_ref, wq, wo, wu, wd, xn, xn2, proj, gated, hidden, part1, core1, chip1, part2, chip2,
           after, ring_send, ring_recv, own_sem, in_sem, fold_send, fold_recv, put_send, put_recv,
           tok_send, tok_recv, gate_send, gate_recv, aside_send, aside_recv, over_send, over_recv, line_send, line_recv,
           swap_send, swap_recv, core1_send, core1_recv, chip1_send, chip1_recv, all_send, all_recv,
           core2_send, core2_recv, chip2_send, chip2_recv):
    half = fs // 2
    lines = fs // 2
    in_refs = (w1_ref, w2_ref, w3_ref, w4_ref)
    deep_q = w1_ref.shape[0]
    chips = tp // 2
    rows = resid_ref.shape[0]
    heads = rate_ref.shape[0]
    tokens = rows * tp
    me_f = lax.axis_index("fs")
    me_t = lax.axis_index("tp")
    pair = me_f % 2
    line = me_f // 2
    other_f = 2 * line + 1 - pair
    chip = me_t // 2
    core = me_t % 2
    other_t = 2 * chip + 1 - core

    def place(i):
        col = i % 2
        at = i // 2
        return at * (1 - col) + (fs - 1 - at) * col

    def index(p):
        col = p // half
        return 2 * (p * (1 - col) + (fs - 1 - p) * col) + col

    my_place = place(me_f)
    target = (index((my_place + 1) % fs), index((my_place + fs - 1) % fs))

    def owner(way, dist):
        if way == 0:
            return index((my_place + fs - dist) % fs)
        return index((my_place + dist) % fs)

    def peer(d):
        return (me_t + d) % tp

    def beside(e):
        return 2 * ((chip + e) % chips) + core

    def step_to(way):
        return me_f + 2 if way == 0 else me_f - 2

    def line_has(way, dist):
        return line >= dist if way == 0 else line + dist <= lines - 1

    def line_next(way):
        return line_has(1 - way, 1)

    upper = line // (lines // 2)
    mate_line = (1 - upper) * (1 - line) + upper * (2 * lines - 3 - line)
    mate_f = 2 * mate_line + pair
    all_fold = lines - 2 == 2
    is_end = jnp.logical_or(line == 0, line == lines - 1)
    inner = jnp.logical_not(is_end)
    folds = inner if all_fold else jnp.logical_or(line == 1, line == lines - 2)
    ring_out = (upper + pair == 1, upper + pair != 1)
    line_out = (upper == 1, upper == 0)

    def when(on, run):
        if on is None:
            run()
        else:
            pl.when(on)(run)

    first_row = pl.multiple_of(me_f * deep_q, deep_q)
    loads = []
    for head in range(heads):
        left = 0
        for ref in in_refs:
            w = ref.shape[1] // heads
            copy = pltpu.make_async_copy(
                ref.at[:, head * w:(head + 1) * w],
                wq.at[head, pl.ds(first_row, deep_q), left:left + w], in_sem.at[len(loads)])
            copy.start()
            loads.append(copy)
            left += w

    barrier = pltpu.get_barrier_semaphore()

    def greet(where):
        pl.semaphore_signal(barrier, inc=1, device_id=where, device_id_type=MESH)

    for way in range(2):
        greet((target[way], me_t))
    for d in range(1, tp):
        greet((me_f, peer(d)))
        if d % 2 == 0:
            greet((other_f, peer(d)))
    greet((other_f, me_t))
    for way in range(2):
        at = (line + (1 if way == 0 else lines - 1)) % lines
        greet((2 * at + pair, me_t))
    pl.semaphore_wait(barrier, 2 + (tp - 1) + (chips - 1) + 1 + 2)

    started = []

    def go(copy, on=None):
        if on is None:
            copy.start()
        else:
            @pl.when(on)
            def _():
                copy.start()
        started.append((copy, on))

    def remote(src, dst, s_sem, r_sem, where):
        return pltpu.make_async_remote_copy(
            src_ref=src, dst_ref=dst, send_sem=s_sem, recv_sem=r_sem, device_id=where,
            device_id_type=MESH)

    def landed(dst, s_sem, r_sem):
        return remote(dst, dst, s_sem, r_sem, (me_f, other_t))

    def span(at, size):
        return pl.ds(pl.multiple_of(at, size), size)

    def half_of(way, turn):
        return turn if way == 0 else 1 - turn

    def ring_rounds(half_ring):
        found = []
        for dist in range(1, half_ring):
            found += [(dist, 0), (dist, 1)]
        return found + [(half_ring, 0)]

    rounds = ring_rounds(half)
    per = len(rounds)
    out_rows = wo_ref.shape[0] // 2

    def slot(who, h):
        return wo.at[who, pl.ds(h * out_rows, out_rows), :]

    ring = []
    for n, (dist, turn) in enumerate(rounds):
        pair_of = []
        for way in range(2):
            h = half_of(way, turn)
            who = owner(way, dist - 1)
            src = wo_ref.at[pl.ds(h * out_rows, out_rows), :] if dist == 1 else slot(who, h)
            pair_of.append((
                remote(src, slot(who, h), ring_send.at[way, n], ring_recv.at[way, n], (target[way], me_t)),
                landed(slot(owner(way, dist), h), ring_send.at[way, n], ring_recv.at[way, n])))
            started.append((pair_of[-1][0], None))
        ring.append(pair_of)

    def send(n, ways=(0, 1), out=None):
        for way in ways:
            copy = ring[n][way][0]
            if out is None:
                copy.start()
            else:
                pl.when(ring_out[way] if out else jnp.logical_not(ring_out[way]))(copy.start)

    def arrive(n, out):
        dist, turn = rounds[n]
        more = dist + 1 < half or (dist + 1 == half and turn == 0)
        for way in range(2):
            def run():
                ring[n][way][1].wait_recv()
                if more:
                    send(n + 2, (way,))
            pl.when(ring_out[way] if out else jnp.logical_not(ring_out[way]))(run)

    count_in = 2 * (lines - 2)
    half_in = count_in // 2

    def place_in(i):
        col = i % 2
        at = i // 2 - 1
        return at * (1 - col) + (count_in - 1 - at) * col

    def index_in(p):
        col = p // half_in
        return 2 * (p * (1 - col) + (count_in - 1 - p) * col + 1) + col

    my_in = (place_in(me_f) + count_in) % count_in
    target_in = (index_in((my_in + 1) % count_in), index_in((my_in + count_in - 1) % count_in))

    def owner_in(way, dist):
        return index_in((my_in + (count_in - dist if way == 0 else dist)) % count_in)

    def mate_of(who):
        at = who // 2
        up = at // (lines // 2)
        return 2 * ((1 - up) * (1 - at) + up * (2 * lines - 3 - at)) + who % 2

    def fold_of(who):
        return jnp.logical_or(who // 2 == 1, who // 2 == lines - 2)

    part_q = deep_q // 2

    def slot_in(head, who, h):
        return wq.at[head, pl.ds(pl.multiple_of(who * deep_q + h * part_q, part_q), part_q), :]

    rounds_in = ring_rounds(half_in)
    per_in = len(rounds_in)
    ring_in = []
    for head in range(heads):
        for s in range(2):
            for dist, turn in rounds_in:
                n = len(ring_in)
                pair_of = []
                for way in range(2):
                    h = half_of(way, turn)
                    gone, come = owner_in(way, dist - 1), owner_in(way, dist)
                    on_out = None if s == 0 or all_fold else fold_of(gone)
                    on_in = None if s == 0 or all_fold else fold_of(come)
                    if s == 1:
                        gone, come = mate_of(gone), mate_of(come)
                    out = remote(slot_in(head, gone, h), slot_in(head, gone, h), fold_send.at[way, n],
                                 fold_recv.at[way, n], (target_in[way], me_t))
                    back = landed(slot_in(head, come, h), fold_send.at[way, n], fold_recv.at[way, n])
                    pair_of.append((out, on_out, back, on_in))
                    started.append((out, inner if on_out is None else jnp.logical_and(inner, on_out)))
                ring_in.append(pair_of)

    def send_in(n):
        for out, on_out, _, _ in ring_in[n]:
            when(on_out, out.start)

    def arrive_in(n):
        for _, _, back, on_in in ring_in[n]:
            when(on_in, back.wait_recv)
        dist, turn = rounds_in[n % per_in]
        if dist + 1 < half_in or (dist + 1 == half_in and turn == 0):
            send_in(n + 2)

    def rows_in(head, who):
        return wq.at[head, pl.ds(pl.multiple_of(who * deep_q, deep_q), deep_q), :]

    puts, puts_in = [], []
    for head in range(heads):
        puts.append(remote(rows_in(head, me_f), rows_in(head, me_f), put_send.at[head], put_recv.at[head],
                           (mate_f, me_t)))
        puts_in.append(landed(rows_in(head, mate_f), put_send.at[head], put_recv.at[head]))
        started.append((puts[-1], is_end))

    up_cols = wu.shape[1]
    deep = wu_ref.shape[0]
    down_rows = wd.shape[1]

    def piece(g, who):
        return wu.at[span(who * deep, deep), :] if g == 0 else wd.at[who]

    def share(g, y):
        if g == 0:
            return wu_ref.at[:, span(y * up_cols, up_cols)]
        return wd_ref.at[span(y * down_rows, down_rows), :]

    line_rounds = [(g, dist, turn) for g in range(2) for dist in range(1, lines) for turn in range(2)]
    per_line = 2 * (lines - 1)

    def line_owner(way, dist, turn):
        at = line - dist if way == 0 else line + dist
        return 2 * at + (pair if turn == 0 else 1 - pair)

    to_end = (line == lines - 2, line == 1)
    line_copies = []
    for m, (g, dist, turn) in enumerate(line_rounds):
        both = []
        for way in range(2):
            who = line_owner(way, dist - 1, turn)
            src = share(g, pair) if dist == 1 and turn == 0 else piece(g, who)
            on = line_next(way) if dist == 1 else jnp.logical_and(line_next(way), line_has(way, dist - 1))
            has = line_has(way, dist)
            if dist == 1 and turn == 1:
                on = jnp.logical_and(on, jnp.logical_not(to_end[way]))
                has = jnp.logical_and(has, inner)
            copy = remote(src, piece(g, who), line_send.at[way, m], line_recv.at[way, m],
                          (step_to(way), me_t))
            back = landed(piece(g, line_owner(way, dist, turn)), line_send.at[way, m],
                          line_recv.at[way, m])
            both.append((copy, on, back, has))
            started.append((copy, on))
        line_copies.append(both)

    def line_send_round(m, ways=(0, 1), out=None):
        for way in ways:
            copy, on, _, _ = line_copies[m][way]
            if out is not None:
                on = jnp.logical_and(on, line_out[way] if out else jnp.logical_not(line_out[way]))
            pl.when(on)(copy.start)

    def line_arrive(m, out):
        g, dist, turn = line_rounds[m]
        for way in range(2):
            def run():
                _, _, back, has = line_copies[m][way]
                pl.when(has)(back.wait_recv)
                if dist + 1 < lines:
                    line_send_round(m + 2, (way,))
            pl.when(line_out[way] if out else jnp.logical_not(line_out[way]))(run)

    aside, aside_in, across_end, across_in = [], [], [], []
    for g in range(2):
        if g == 0:
            stash = xn.at[tokens:tokens + deep, :up_cols]
        else:
            stash = xn.at[tokens:tokens + down_rows, up_cols:up_cols + wd.shape[2]]
        aside.append(remote(share(g, 1 - pair), stash, aside_send.at[g], aside_recv.at[g], (mate_f, me_t)))
        aside_in.append(landed(stash, aside_send.at[g], aside_recv.at[g]))
        across_end.append(remote(stash, piece(g, mate_f), over_send.at[g], over_recv.at[g], (other_f, me_t)))
        across_in.append(landed(piece(g, 2 * mate_line + 1 - pair), over_send.at[g], over_recv.at[g]))
        started.append((aside[-1], folds))
        started.append((across_end[-1], is_end))

    swaps, swaps_in = [], []
    for g in range(2):
        swaps.append(remote(share(g, 1 - pair), piece(g, me_f), swap_send.at[g], swap_recv.at[g],
                            (other_f, me_t)))
        swaps_in.append(landed(piece(g, other_f), swap_send.at[g], swap_recv.at[g]))
        started.append((swaps[-1], None))

    own = [None]
    for n, (src, dst) in enumerate((
            (wo_ref, wo.at[me_f]),
            (share(0, pair), piece(0, me_f)),
            (share(1, pair), piece(1, me_f)))):
        copy = pltpu.make_async_copy(src, dst, own_sem.at[n])
        own.append(copy)

    my_rows = span(me_t * rows, rows)

    def norm(source, gain_ref):
        wide = source.astype(F32)
        mean = jnp.mean(wide * wide, axis=-1, keepdims=True)
        return (wide * lax.rsqrt(mean + EPS) * gain_ref[...]).astype(BF16)

    step = 64

    def norm_into(buf, first, source_ref, gain_ref):
        @pl.loop(0, rows // step)
        def _(i):
            at = pl.multiple_of(i * step, step)
            buf[pl.ds(pl.multiple_of(first + at, step), step), :] = norm(
                source_ref[pl.ds(at, step), :], gain_ref)

    half_rows = rows // 2

    def tok(group, t, part=None):
        first = group * tokens + t * rows
        if part is None:
            return xn.at[span(first, rows), :]
        return xn.at[pl.ds(pl.multiple_of(first + part * half_rows, half_rows), half_rows), :]

    xn_sends = []
    tok_count = [0]

    def tok_pair(out_ref, in_ref, where, on):
        n = tok_count[0]
        tok_count[0] += 1
        out = remote(out_ref, out_ref, tok_send.at[n], tok_recv.at[n], where)
        xn_sends.append((out, on))
        return out, landed(in_ref, tok_send.at[n], tok_recv.at[n])

    def tok_set(group, part, on):
        core_c = tok_pair(tok(group, me_t, part), tok(group, other_t, part), (me_f, other_t), on)
        over, pass_on = [], []
        for e in range(1, chips):
            t = beside(chips - e)
            over.append(tok_pair(tok(group, me_t, part), tok(group, t, part), (me_f, beside(e)), on))
            pass_on.append(tok_pair(
                tok(group, t, part),
                tok(group, 2 * ((chip + chips - e) % chips) + 1 - core, part), (me_f, other_t), on))
        return core_c, over, pass_on

    own_set = tok_set(1, None, inner)
    mate_sets = [tok_set(0, part, folds) for part in range(2)]
    to_mate = [tok_pair(tok(0, me_t, part), tok(0, me_t, part), (mate_f, me_t), is_end) for part in range(2)]

    def tok_start(which):
        which[0][0].start()
        for out, _ in which[1]:
            out.start()

    def tok_pass(which):
        for (_, back), (out, _) in zip(which[1], which[2]):
            back.wait_recv()
            out.start()

    def tok_wait(which):
        which[0][1].wait_recv()
        for _, back in which[2]:
            back.wait_recv()

    def mate_tokens(part):
        def run():
            to_mate[part][1].wait_recv()
            tok_start(mate_sets[part])
        return lambda: when(None if all_fold else folds, run)

    def mate_pass(part):
        return lambda: when(None if all_fold else folds, lambda: tok_pass(mate_sets[part]))

    gates, gates_in = [], []
    for head in range(heads):
        cut = slice(head * DV, (head + 1) * DV)
        gates.append(remote(gated.at[0, :, cut], gated.at[1, :, cut], gate_send.at[head], gate_recv.at[head],
                            (mate_f, me_t)))
        gates_in.append(landed(gated.at[1, :, cut], gate_send.at[head], gate_recv.at[head]))
        started.append((gates[-1], folds))

    def project(group, head):
        width = proj.shape[1]
        t = tile_of(width)

        @pl.loop(0, width // t)
        def _(j):
            cols = pl.ds(pl.multiple_of(j * t, t), t)
            proj[:, cols] = jnp.dot(xn[group * tokens:(group + 1) * tokens, :], wq[head, :, cols],
                                    preferred_element_type=F32).astype(BF16)

    def retain(group, head):
        rate = rate_ref[head]

        @pl.loop(0, tokens // LENGTH)
        def _(n):
            base = pl.multiple_of(n * LENGTH, LENGTH)
            rs = pl.ds(base, LENGTH)
            q = proj[rs, :DK]
            k = proj[rs, DK:2 * DK]
            v = proj[rs, 2 * DK:2 * DK + DV]
            g = proj[rs, 2 * DK + DV:].astype(F32)
            scores = lax.dot_general(q, k, (((1,), (1,)), ((), ())), preferred_element_type=F32)
            t_at = lax.broadcasted_iota(jnp.int32, (LENGTH, LENGTH), 0)
            s_at = lax.broadcasted_iota(jnp.int32, (LENGTH, LENGTH), 1)
            gap = t_at - s_at
            decay = jnp.exp(-rate * jnp.maximum(gap, 0).astype(F32)) * (DK ** -0.5)
            scores = jnp.where(gap >= 0, scores * decay, 0.0).astype(BF16)
            mixed = jnp.dot(scores, v, preferred_element_type=F32)
            mean = jnp.mean(mixed, axis=-1, keepdims=True)
            off = mixed - mean
            var = jnp.mean(off * off, axis=-1, keepdims=True)
            grouped = off * lax.rsqrt(var + EPS)
            gated[group, rs, head * DV:(head + 1) * DV] = (g / (1.0 + jnp.exp(-g)) * grouped).astype(BF16)

    def heads_of(group, head):
        project(group, head)
        retain(group, head)
        if group == 0:
            gates[head].start()

    def mate_heads(head):
        when(None if all_fold else folds, lambda: heads_of(0, head))

    def mix_block(x, c):
        return part1.at[span((2 * x + c) * rows, rows), :]

    def mix_out():
        cols = wo.shape[2]

        @pl.loop(0, fs)
        def _(j):
            part1[:, span(j * cols, cols)] = jnp.dot(
                gated[1], wo[j], preferred_element_type=F32).astype(BF16)
        order = [e % chips for e in range(1, chips + 1)]
        for e in order:
            x = (chip + e) % chips
            go(remote(mix_block(x, 1 - core), core1.at[e], core1_send.at[e], core1_recv.at[e],
                      (me_f, other_t)))
        for e in order:
            landed(core1.at[e], core1_send.at[e], core1_recv.at[e]).wait_recv()
            if e:
                first = beside(e) * rows

                @pl.loop(0, rows // step)
                def _(i):
                    at = pl.ds(pl.multiple_of(first + i * step, step), step)
                    more = core1[e, span(i * step, step), :].astype(F32)
                    part1[at, :] = (part1[at, :].astype(F32) + more).astype(BF16)
                go(remote(ag_mix(beside(e)), chip1.at[e - 1], chip1_send.at[e - 1],
                          chip1_recv.at[e - 1], (me_f, beside(e))))

    def ag_mix(t):
        return part1.at[span(t * rows, rows), :]

    def mix_end():
        for e in range(1, chips):
            landed(chip1.at[e - 1], chip1_send.at[e - 1], chip1_recv.at[e - 1]).wait_recv()

        @pl.loop(0, rows // step)
        def _(i):
            at = span(i * step, step)
            total = part1[pl.ds(pl.multiple_of(me_t * rows + i * step, step), step), :].astype(F32)
            total = total + core1[0, at, :].astype(F32)
            for e in range(1, chips):
                total = total + chip1[e - 1, at, :].astype(F32)
            sum_ = (resid_ref[at, :].astype(F32) + total).astype(BF16)
            after[at, :] = sum_
            xn2[pl.ds(pl.multiple_of(block(pair, me_t) * rows + i * step, step), step), :] = norm(
                sum_, mlp_gain_ref)

    def block(y, t):
        return (t % 2) * (2 * chips) + y * chips + t // 2

    def wide(y, t, part=None):
        first = block(y, t) * rows
        hr = rows // 2
        if part is None:
            return xn2.at[span(first, rows), :]
        return xn2.at[pl.ds(pl.multiple_of(first + part * hr, hr), hr), :]

    more_chips = chips - 1
    pieces = 1 + 3 * more_chips

    def all_copy(n, ref, where):
        go(remote(ref, ref, all_send.at[n], all_recv.at[n], where))

    def all_landed(n, ref):
        landed(ref, all_send.at[n], all_recv.at[n]).wait_recv()

    def across(n, ref):
        all_copy(pieces + n, ref, (me_f, other_t))

    def all_first():
        ref = wide(pair, me_t)
        all_copy(0, ref, (other_f, me_t))
        for e in range(1, chips):
            all_copy(e, ref, (me_f, beside(e)))
        all_copy(2 * pieces, ref, (me_f, other_t))

    def all_second():
        ref = wide(1 - pair, me_t)
        all_landed(0, ref)
        for e in range(1, chips):
            all_copy(more_chips + e, wide(1 - pair, me_t, 0), (me_f, beside(e)))
        across(0, ref)
        for e in range(1, chips):
            t = beside(chips - e)
            all_landed(e, wide(pair, t))
            all_copy(2 * more_chips + e, wide(pair, t, 1), (other_f, me_t))
            across(e, wide(pair, t))

    def all_beside():
        all_landed(2 * pieces, wide(pair, other_t))
        for e in range(1, chips):
            t = 2 * ((chip + chips - e) % chips) + 1 - core
            all_landed(pieces + e, wide(pair, t))

    def all_third():
        for part in range(2):
            for e in range(1, chips):
                n = (1 + part) * more_chips + e
                ref = wide(1 - pair, beside(chips - e), part)
                all_landed(n, ref)
                across(n, ref)
        all_landed(pieces, wide(1 - pair, other_t))
        for e in range(1, chips):
            t = 2 * ((chip + chips - e) % chips) + 1 - core
            for part in range(2):
                all_landed(pieces + (1 + part) * more_chips + e, wide(1 - pair, t, part))

    def lift(y):
        t = tile_of(up_cols)
        size = chips * rows

        @pl.loop(0, up_cols // t)
        def _(j):
            cols = span(j * t, t)

            @pl.loop(0, 2)
            def _(i):
                at = span(i * tokens + y * size, size)
                up = jnp.maximum(jnp.dot(xn2[at, :], wu[:, cols], preferred_element_type=F32), 0.0)
                hidden[at, cols] = (up * up).astype(BF16)

    cw = wd.shape[2]
    r2 = 2 * chips - 1

    def lower_copy(who, n, ref, where):
        dst = chip2.at[n, :, span(who * cw, cw)]
        out = remote(ref, dst, chip2_send.at[n, who], chip2_recv.at[n, who], where)
        return out, landed(dst, chip2_send.at[n, who], chip2_recv.at[n, who])

    def part_rows(y, t):
        return span(block(y, t) * rows, rows)

    def along_chips(who, cols):
        first, second = [], []
        for e in range(1, chips):
            for y in range(2):
                first.append(lower_copy(who, 2 * (e - 1) + y, part2.at[part_rows(y, beside(e)), cols],
                                        (me_f, beside(e))))
        second.append(lower_copy(who, r2 - 1, part2.at[part_rows(1 - pair, me_t), cols], (other_f, me_t)))

        def add():
            at = part_rows(1 - pair, me_t)
            total = part2[at, cols].astype(F32)
            for e in range(1, chips):
                total = total + chip2[2 * (e - 1) + 1 - pair, :, cols].astype(F32)
            part2[at, cols] = total.astype(BF16)

        def rest():
            total = chip2[r2 - 1, :, cols].astype(F32)
            for e in range(1, chips):
                total = total + chip2[2 * (e - 1) + pair, :, cols].astype(F32)
            return total
        return first, second, add, rest

    def across_pair(who, cols):
        first, second = [], []
        for e in range(chips):
            first.append(lower_copy(who, e, part2.at[part_rows(1 - pair, beside(e)), cols], (other_f, me_t)))
        for e in range(1, chips):
            second.append(lower_copy(who, chips + e - 1, part2.at[part_rows(pair, beside(e)), cols],
                                     (me_f, beside(e))))

        def add():
            for e in range(1, chips):
                at = part_rows(pair, beside(e))
                part2[at, cols] = (part2[at, cols].astype(F32) + chip2[e, :, cols].astype(F32)).astype(BF16)

        def rest():
            total = chip2[0, :, cols].astype(F32)
            for e in range(1, chips):
                total = total + chip2[chips + e - 1, :, cols].astype(F32)
            return total
        return first, second, add, rest

    finals, middles = [], []

    def lower(who, on=None):
        cols = span(who * cw, cw)
        mine = part_rows(pair, me_t)
        side = remote(part2.at[span((1 - core) * tokens, tokens), cols], xn.at[pl.ds(0, tokens), cols],
                      core2_send.at[who], core2_recv.at[who], (me_f, other_t))
        side_in = landed(xn.at[pl.ds(0, tokens), cols], core2_send.at[who], core2_recv.at[who])
        plans = [(who % 2 == 0, along_chips(who, cols)), (who % 2 == 1, across_pair(who, cols))]

        def run():
            @pl.loop(0, 2)
            def _(i):
                at = span(((1 - core) * (1 - i) + core * i) * tokens, tokens)
                part2[at, cols] = jnp.dot(
                    hidden[at, :], wd[who], preferred_element_type=F32).astype(BF16)

                @pl.when(i == 0)
                def _():
                    side.start()
            side_in.wait_recv()

            @pl.loop(0, tokens // 128)
            def _(i):
                at = pl.ds(pl.multiple_of(core * tokens + i * 128, 128), 128)
                more = xn[span(i * 128, 128), cols].astype(F32)
                part2[at, cols] = (part2[at, cols].astype(F32) + more).astype(BF16)
            for this, (first, _, _, _) in plans:
                def begin():
                    for out, _ in first:
                        out.start()
                pl.when(this)(begin)

        def middle():
            for this, (first, second, add, _) in plans:
                def pass_on():
                    for _, back in first:
                        back.wait_recv()
                    add()
                    for out, _ in second:
                        out.start()
                pl.when(this)(pass_on)

        def end():
            for this, (first, second, _, rest) in plans:
                def close():
                    for _, back in second:
                        back.wait_recv()
                    total = part2[mine, cols].astype(F32) + rest()
                    out_ref[:, cols] = (after[:, cols].astype(F32) + total).astype(BF16)
                    for out, _ in first + second:
                        out.wait_send()
                pl.when(this)(close)
            side.wait_send()

        when(on, run)
        middles.append((middle, on))
        finals.append((end, on))
        if len(middles) > 2:
            then, at = middles[-3]
            when(at, then)

    if all_fold:
        inner_order = [[(0, False), (1, False), (0, True), (1, True)],
                       [(2, False), (3, False), (2, True), (3, True)], [(4, False), (5, False)],
                       [(4, True), (5, True)], [(6, True), (6, False)]]
        end_order = [[(0, False), (1, False), (0, True), (1, True), (2, False), (3, False)],
                     [(2, True), (3, True), (4, False)], [(5, False), (4, True), (5, True), (6, True), (6, False)]]
    else:
        by_round = [(n, out) for n in range(per) for out in (False, True)]
        inner_order = [[], [], [], [], by_round]
        end_order = [[], [], by_round]

    def arrivals(part):
        for n, out in part:
            arrive(n, out)

    def inner_front():
        send(0, out=True)
        send(1, out=True)
        line_send_round(0, out=True)

        when(None if all_fold else folds, aside[0].start)
        line_send_round(per_line, out=True)
        when(None if all_fold else folds, aside[1].start)
        for copy in loads:
            copy.wait()
        send_in(0)
        send_in(1)
        norm_into(xn, tokens + me_t * rows, resid_ref, mix_gain_ref)
        tok_start(own_set)
        for copy in own[1:]:
            copy.start()
        hooks = {(0, 1, 0): mate_tokens(0), (0, 1, 1): lambda: tok_pass(own_set),
                 (1, 0, 0): mate_tokens(1), (1, 0, 2): mate_pass(0), (1, 1, 0): mate_pass(1)}
        order = list(hooks)

        def drain(upto):
            while order and order[0] <= upto:
                hooks[order.pop(0)]()

        for head in range(heads):
            last = head == heads - 1
            first = 2 * head * per_in
            for n in range(per_in):
                arrive_in(first + n)
                drain((head, 0, n))
                if n == 1:
                    if last:
                        send(0, out=False)
                        send(1, out=False)

                    def pushed():
                        puts_in[head].wait_recv()
                    when(None if all_fold else folds, pushed)
                    send_in(first + per_in)
                    send_in(first + per_in + 1)
            for n in range(per_in):
                arrive_in(first + per_in + n)
                if n == 0:
                    if last:
                        for g in range(2):
                            swaps[g].start()
                        arrivals(inner_order[0])
                    else:
                        send_in(first + 2 * per_in)
                        send_in(first + 2 * per_in + 1)
                drain((head, 1, n))
                if n == 0 and last:
                    drain((2, 0, 0))
                    for part in range(2):
                        when(None if all_fold else folds, lambda: tok_wait(mate_sets[part]))
                    for early in range(head):
                        mate_heads(early)
                    arrivals(inner_order[1])
            if not last:
                if head == 0:
                    tok_wait(own_set)
                heads_of(1, head)
        if heads == 1:
            tok_wait(own_set)
        arrivals(inner_order[2])
        line_send_round(0, out=False)
        mate_heads(heads - 1)
        arrivals(inner_order[3])
        swaps_in[0].wait_recv()
        line_send_round(1)
        heads_of(1, heads - 1)
        arrivals(inner_order[4])

    def end_front():
        send(0, out=True)
        send(1, out=True)
        for g in range(2):
            swaps[g].start()
        for copy in loads:
            copy.wait()
        puts[0].start()
        norm_into(xn, me_t * rows, resid_ref, mix_gain_ref)
        for out, _ in to_mate:
            out.start()
        for head in range(1, heads):
            puts[head].start()
        send(0, out=False)
        send(1, out=False)
        for copy in own[1:]:
            copy.start()
        arrivals(end_order[0])
        swaps_in[0].wait_recv()
        aside_in[0].wait_recv()
        across_end[0].start()
        line_send_round(0)
        arrivals(end_order[1])
        line_send_round(1)
        aside_in[1].wait_recv()
        across_end[1].start()
        line_send_round(per_line)
        swaps_in[1].wait_recv()
        line_send_round(per_line + 1)
        arrivals(end_order[2])
        for back in gates_in:
            back.wait_recv()

    pl.when(inner)(inner_front)
    pl.when(is_end)(end_front)
    own[1].wait()
    mix_out()
    line_arrive(0, False)
    line_arrive(1, False)

    def inner_down():
        line_send_round(per_line, out=False)
        swaps_in[1].wait_recv()
        line_send_round(per_line + 1)
    pl.when(inner)(inner_down)

    line_arrive(0, True)
    line_arrive(1, True)
    for copy, on in xn_sends:
        pl.when(on)(copy.wait_send)
    mix_end()
    all_first()
    line_arrive(2, False)
    line_arrive(3, False)
    line_arrive(2, True)
    line_arrive(3, True)
    all_second()
    for k in range(4, per_line):
        line_arrive(k, False)
        line_arrive(k, True)
    for k in range(2):
        line_arrive(per_line + k, False)

    def end_landed():
        for back in across_in:
            back.wait_recv()
    pl.when(is_end)(end_landed)
    line_arrive(per_line, True)
    own[2].wait()
    own[3].wait()
    all_beside()
    lift(pair)
    all_third()
    line_arrive(per_line + 1, True)
    lift(1 - pair)
    lower(me_f)
    lower(other_f)
    for m in range(per_line, 2 * per_line):
        if m + 2 < 2 * per_line:
            line_arrive(m + 2, False)
        _, dist, turn = line_rounds[m]
        if m >= per_line + 2:
            line_arrive(m, True)
        for way in range(2):
            lower(line_owner(way, dist, turn), line_has(way, dist))

    for then, on in middles[-2:]:
        when(on, then)
    for end, on in finals:
        when(on, end)
    for copy, on in started:
        when(on, copy.wait_send)


def on_device(fs, tp, resid, mix_gain, w_query, w_key, w_value, w_gate, w_output, decay_rate,
              mlp_gain, w_up, w_down):
    rows, width = resid.shape
    tokens = rows * tp
    in_width = w_query.shape[1] + w_key.shape[1] + w_value.shape[1] + w_gate.shape[1]
    chips = tp // 2
    heads = decay_rate.shape[0]
    wide = 2 * (1 + 3 * (chips - 1)) + 1
    vmem = pl.BlockSpec(memory_space=pltpu.VMEM)
    hbm = pl.BlockSpec(memory_space=pl.ANY)
    dma = pltpu.SemaphoreType.DMA
    cols = width // fs
    return pl.pallas_call(
        functools.partial(kernel, fs, tp),
        out_shape=jax.ShapeDtypeStruct((rows, width), BF16),
        in_specs=[vmem] * 3 + [pl.BlockSpec(memory_space=pltpu.SMEM)] + [hbm] * 7,
        out_specs=vmem,
        scratch_shapes=[
            pltpu.VMEM((heads, width, in_width // heads), BF16),
            pltpu.VMEM((fs, w_output.shape[0], cols), BF16),
            pltpu.VMEM((width, w_up.shape[1] // 2), BF16),
            pltpu.VMEM((fs, w_down.shape[0] // 2, cols), BF16),
            pltpu.VMEM((2 * tokens, width), BF16),
            pltpu.VMEM((2 * tokens, width), BF16),
            pltpu.VMEM((tokens, in_width // heads), BF16),
            pltpu.VMEM((2, tokens, w_output.shape[0]), BF16),
            pltpu.VMEM((2 * tokens, w_up.shape[1] // 2), BF16),
            pltpu.VMEM((tokens, width), BF16),
            pltpu.VMEM((chips, rows, width), BF16),
            pltpu.VMEM((chips - 1, rows, width), BF16),
            pltpu.VMEM((2 * tokens, width), BF16),
            pltpu.VMEM((2 * chips - 1, rows, width), BF16),
            pltpu.VMEM((rows, width), BF16),
            dma((2, fs - 1)),
            dma((2, fs - 1)),
            dma((3,)),
            dma((4 * heads,)),
            dma((2, 2 * heads * (fs - 5))),
            dma((2, 2 * heads * (fs - 5))),
            dma((heads,)),
            dma((heads,)),
            dma((3 * (2 * chips - 1) + 2,)),
            dma((3 * (2 * chips - 1) + 2,)),
            dma((heads,)),
            dma((heads,)),
            dma((2,)),
            dma((2,)),
            dma((2,)),
            dma((2,)),
            dma((2, 2 * (fs - 2))),
            dma((2, 2 * (fs - 2))),
            dma((2,)),
            dma((2,)),
            dma((chips,)),
            dma((chips,)),
            dma((chips - 1,)),
            dma((chips - 1,)),
            dma((wide,)),
            dma((wide,)),
            dma((fs,)),
            dma((fs,)),
            dma((2 * chips - 1, fs)),
            dma((2 * chips - 1, fs)),
        ],
        compiler_params=pltpu.CompilerParams(
            collective_id=0, has_side_effects=True, vmem_limit_bytes=67043328),
    )(resid, mix_gain[None, :], mlp_gain[None, :], decay_rate, w_query, w_key, w_value,
      w_gate, w_output, w_up, w_down)


def solution(mesh):
    placed = (
        P(("fs", "tp"), None),
        P(),
        P("fs", "tp"),
        P("fs", "tp"),
        P("fs", "tp"),
        P("fs", "tp"),
        P("tp", "fs"),
        P("tp"),
        P(),
        P("fs", "tp"),
        P("tp", "fs"),
    )
    sizes = dict(mesh.shape)
    return jax.shard_map(
        functools.partial(on_device, sizes["fs"], sizes["tp"]), mesh=mesh, in_specs=placed,
        out_specs=P(("fs", "tp"), None), check_vma=False)
```

time: 243 us -> 232 us (0.955)
  Pallas kernels: 241 us -> 229 us
    pallas_call x1, Pallas kernels: 241 us -> 229 us  [on_device(): pl.pallas_call(functools.partial(kernel, fs, tp), out_shape=jax.ShapeDtyp...]
where the time goes in v1:
time: 232 us
  Pallas kernels  229 us (99%)
    pallas_call x1, Pallas kernels, on_device(): pl.pallas_call(functools.partial(kernel, fs, tp), out_shape=jax.ShapeDtyp...  229 us

profile of v1, /device:TPU:0, one launch (start us, length us, event | category | flops | bytes accessed | tf_op | source)
XLA Modules:
  0.0 231.6 jit_solution(16441057594065155223)
XLA Ops:
  0.0 229.3 %shard_map.109 = bf16[256,2048]{1,0:T(8,128)(2,1)} custom-call(bf16[256,2048]{1,0:T(8,128)(2,1)} %resid_ref.1, f32[1,2048]{1,0:T(1,128)} %bitcast.2, f32[1,2048]{1,0:T(1,128)} %bitcast.3, f32[2]{0:T(128)} %rate_ref.1, bf16[256,256]{1,0:T(8,128)(2,1)} %w1_ref.1, bf16[256,256]{1,0:T(8,128)(2,1)} %w2_ref.1, bf16[256,512]{1,0:T(8,128)(2,1)} %w3_ref.1, ...), custom_call_target="tpu_custom_call" | custom-call | tf_op jit(solution)/shard_map/pallas_call | solution.py:905
  229.3 2.3 copy.13

commit v2 on v1

--- a/solution.py
+++ b/solution.py
@@ -12,6 +12,7 @@
 LENGTH = 512
 MESH = pl.DeviceIdType.MESH
 EPS = 1e-06
+CHUNKS = 8
 F32 = jnp.float32
 BF16 = jnp.bfloat16
 
@@ -28,6 +29,7 @@
            core2_send, core2_recv, chip2_send, chip2_recv):
     half = fs // 2
     lines = fs // 2
+    chunks = CHUNKS
     in_refs = (w1_ref, w2_ref, w3_ref, w4_ref)
     deep_q = w1_ref.shape[0]
     chips = tp // 2
@@ -472,6 +474,8 @@
     def mate_heads(head):
         when(None if all_fold else folds, lambda: heads_of(0, head))
 
+    size = rows // chunks
+
     def mix_block(x, c):
         return part1.at[span((2 * x + c) * rows, rows), :]
 
@@ -490,98 +494,93 @@
         for e in order:
             landed(core1.at[e], core1_send.at[e], core1_recv.at[e]).wait_recv()
             if e:
-                first = beside(e) * rows
-
-                @pl.loop(0, rows // step)
-                def _(i):
-                    at = pl.ds(pl.multiple_of(first + i * step, step), step)
-                    more = core1[e, span(i * step, step), :].astype(F32)
+                for c in range(chunks):
+                    at = pl.ds(pl.multiple_of(beside(e) * rows + c * size, size), size)
+                    here = slice(c * size, (c + 1) * size)
+                    more = core1[e, here, :].astype(F32)
                     part1[at, :] = (part1[at, :].astype(F32) + more).astype(BF16)
-                go(remote(ag_mix(beside(e)), chip1.at[e - 1], chip1_send.at[e - 1],
-                          chip1_recv.at[e - 1], (me_f, beside(e))))
-
-    def ag_mix(t):
-        return part1.at[span(t * rows, rows), :]
-
-    def mix_end():
-        for e in range(1, chips):
-            landed(chip1.at[e - 1], chip1_send.at[e - 1], chip1_recv.at[e - 1]).wait_recv()
-
-        @pl.loop(0, rows // step)
-        def _(i):
-            at = span(i * step, step)
-            total = part1[pl.ds(pl.multiple_of(me_t * rows + i * step, step), step), :].astype(F32)
-            total = total + core1[0, at, :].astype(F32)
-            for e in range(1, chips):
-                total = total + chip1[e - 1, at, :].astype(F32)
-            sum_ = (resid_ref[at, :].astype(F32) + total).astype(BF16)
-            after[at, :] = sum_
-            xn2[pl.ds(pl.multiple_of(block(pair, me_t) * rows + i * step, step), step), :] = norm(
-                sum_, mlp_gain_ref)
+                    n = (e - 1) * chunks + c
+                    go(remote(part1.at[at, :], chip1.at[e - 1, here, :], chip1_send.at[n],
+                              chip1_recv.at[n], (me_f, beside(e))))
 
     def block(y, t):
-        return (t % 2) * (2 * chips) + y * chips + t // 2
-
-    def wide(y, t, part=None):
-        first = block(y, t) * rows
-        hr = rows // 2
-        if part is None:
-            return xn2.at[span(first, rows), :]
-        return xn2.at[pl.ds(pl.multiple_of(first + part * hr, hr), hr), :]
-
-    more_chips = chips - 1
-    pieces = 1 + 3 * more_chips
-
-    def all_copy(n, ref, where):
-        go(remote(ref, ref, all_send.at[n], all_recv.at[n], where))
-
-    def all_landed(n, ref):
-        landed(ref, all_send.at[n], all_recv.at[n]).wait_recv()
-
-    def across(n, ref):
-        all_copy(pieces + n, ref, (me_f, other_t))
-
-    def all_first():
-        ref = wide(pair, me_t)
-        all_copy(0, ref, (other_f, me_t))
-        for e in range(1, chips):
-            all_copy(e, ref, (me_f, beside(e)))
-        all_copy(2 * pieces, ref, (me_f, other_t))
-
-    def all_second():
-        ref = wide(1 - pair, me_t)
-        all_landed(0, ref)
-        for e in range(1, chips):
-            all_copy(more_chips + e, wide(1 - pair, me_t, 0), (me_f, beside(e)))
-        across(0, ref)
+        return (t % 2) * (2 * chips) + (t // 2) * 2 + y
+
+    def wide(y, t, c):
+        return xn2.at[pl.ds(pl.multiple_of(block(y, t) * rows + c * size, size), size), :]
+
+    all_count = [0]
+
+    def all_pair(out_ref, in_ref, where):
+        n = all_count[0]
+        all_count[0] += 1
+        out = remote(out_ref, out_ref, all_send.at[n], all_recv.at[n], where)
+        started.append((out, None))
+        return out, landed(in_ref, all_send.at[n], all_recv.at[n])
+
+    to_core, to_pair, to_chip, pair_core, chip_core, corner, corner_core = [], [], [], [], [], [], []
+    for c in range(chunks):
+        to_core.append(all_pair(wide(pair, me_t, c), wide(pair, other_t, c), (me_f, other_t)))
+        to_pair.append(all_pair(wide(pair, me_t, c), wide(1 - pair, me_t, c), (other_f, me_t)))
+        pair_core.append(all_pair(wide(1 - pair, me_t, c), wide(1 - pair, other_t, c), (me_f, other_t)))
+        for found in (to_chip, chip_core, corner, corner_core):
+            found.append([])
         for e in range(1, chips):
             t = beside(chips - e)
-            all_landed(e, wide(pair, t))
-            all_copy(2 * more_chips + e, wide(pair, t, 1), (other_f, me_t))
-            across(e, wide(pair, t))
-
-    def all_beside():
-        all_landed(2 * pieces, wide(pair, other_t))
+            t_other = 2 * ((chip + chips - e) % chips) + 1 - core
+            to_chip[c].append(all_pair(wide(pair, me_t, c), wide(pair, t, c), (me_f, beside(e))))
+            chip_core[c].append(all_pair(wide(pair, t, c), wide(pair, t_other, c), (me_f, other_t)))
+            if c < chunks - 1:
+                corner[c].append(all_pair(wide(pair, t, c), wide(1 - pair, t, c), (other_f, me_t)))
+            else:
+                corner[c].append(all_pair(wide(1 - pair, me_t, c), wide(1 - pair, t, c), (me_f, beside(e))))
+            corner_core[c].append(all_pair(wide(1 - pair, t, c), wide(1 - pair, t_other, c), (me_f, other_t)))
+
+    def mix_chunk(c):
+        here = slice(c * size, (c + 1) * size)
         for e in range(1, chips):
-            t = 2 * ((chip + chips - e) % chips) + 1 - core
-            all_landed(pieces + e, wide(pair, t))
-
-    def all_third():
-        for part in range(2):
-            for e in range(1, chips):
-                n = (1 + part) * more_chips + e
-                ref = wide(1 - pair, beside(chips - e), part)
-                all_landed(n, ref)
-                across(n, ref)
-        all_landed(pieces, wide(1 - pair, other_t))
+            n = (e - 1) * chunks + c
+            landed(chip1.at[e - 1, here, :], chip1_send.at[n], chip1_recv.at[n]).wait_recv()
+        total = part1[pl.ds(pl.multiple_of(me_t * rows + c * size, size), size), :].astype(F32)
+        total = total + core1[0, here, :].astype(F32)
         for e in range(1, chips):
-            t = 2 * ((chip + chips - e) % chips) + 1 - core
-            for part in range(2):
-                all_landed(pieces + (1 + part) * more_chips + e, wide(1 - pair, t, part))
-
-    def lift(y):
+            total = total + chip1[e - 1, here, :].astype(F32)
+        sum_ = (resid_ref[here, :].astype(F32) + total).astype(BF16)
+        after[here, :] = sum_
+        xn2[pl.ds(pl.multiple_of(block(pair, me_t) * rows + c * size, size), size), :] = norm(
+            sum_, mlp_gain_ref)
+        to_pair[c][0].start()
+        for out, _ in to_chip[c]:
+            out.start()
+        to_core[c][0].start()
+
+    def take_pair(c):
+        to_pair[c][1].wait_recv()
+        if c == chunks - 1:
+            for out, _ in corner[c]:
+                out.start()
+        pair_core[c][0].start()
+
+    def take_chip(c):
+        for n in range(chips - 1):
+            to_chip[c][n][1].wait_recv()
+            if c < chunks - 1:
+                corner[c][n][0].start()
+            chip_core[c][n][0].start()
+
+    def take_corner(c):
+        for n in range(chips - 1):
+            corner[c][n][1].wait_recv()
+            corner_core[c][n][0].start()
+
+    def take_core(found):
+        for c in range(chunks):
+            for _, back in (found[c] if isinstance(found[c], list) else [found[c]]):
+                back.wait_recv()
+
+    def lift(x, y=None):
         t = tile_of(up_cols)
-        size = chips * rows
+        deep_x = 2 * rows if y is None else rows
 
         @pl.loop(0, up_cols // t)
         def _(j):
@@ -589,17 +588,17 @@
 
             @pl.loop(0, 2)
             def _(i):
-                at = span(i * tokens + y * size, size)
+                at = span(i * tokens + 2 * x * rows + (0 if y is None else y * rows), deep_x)
                 up = jnp.maximum(jnp.dot(xn2[at, :], wu[:, cols], preferred_element_type=F32), 0.0)
                 hidden[at, cols] = (up * up).astype(BF16)
 
     cw = wd.shape[2]
     r2 = 2 * chips - 1
 
-    def lower_copy(who, n, ref, where):
-        dst = chip2.at[n, :, span(who * cw, cw)]
-        out = remote(ref, dst, chip2_send.at[n, who], chip2_recv.at[n, who], where)
-        return out, landed(dst, chip2_send.at[n, who], chip2_recv.at[n, who])
+    def lower_copy(who, cols, n, ref, where, base=0):
+        dst = chip2.at[n, :, cols]
+        out = remote(ref, dst, chip2_send.at[base + n, who], chip2_recv.at[base + n, who], where)
+        return out, landed(dst, chip2_send.at[base + n, who], chip2_recv.at[base + n, who])
 
     def part_rows(y, t):
         return span(block(y, t) * rows, rows)
@@ -608,9 +607,9 @@
         first, second = [], []
         for e in range(1, chips):
             for y in range(2):
-                first.append(lower_copy(who, 2 * (e - 1) + y, part2.at[part_rows(y, beside(e)), cols],
+                first.append(lower_copy(who, cols, 2 * (e - 1) + y, part2.at[part_rows(y, beside(e)), cols],
                                         (me_f, beside(e))))
-        second.append(lower_copy(who, r2 - 1, part2.at[part_rows(1 - pair, me_t), cols], (other_f, me_t)))
+        second.append(lower_copy(who, cols, r2 - 1, part2.at[part_rows(1 - pair, me_t), cols], (other_f, me_t)))
 
         def add():
             at = part_rows(1 - pair, me_t)
@@ -629,10 +628,11 @@
     def across_pair(who, cols):
         first, second = [], []
         for e in range(chips):
-            first.append(lower_copy(who, e, part2.at[part_rows(1 - pair, beside(e)), cols], (other_f, me_t)))
+            first.append(lower_copy(who, cols, e, part2.at[part_rows(1 - pair, beside(e)), cols],
+                                    (other_f, me_t), r2))
         for e in range(1, chips):
-            second.append(lower_copy(who, chips + e - 1, part2.at[part_rows(pair, beside(e)), cols],
-                                     (me_f, beside(e))))
+            second.append(lower_copy(who, cols, chips + e - 1, part2.at[part_rows(pair, beside(e)), cols],
+                                     (me_f, beside(e)), r2))
 
         def add():
             for e in range(1, chips):
@@ -646,7 +646,19 @@
             return total
         return first, second, add, rest
 
-    finals, middles = [], []
+    finals, joins, middles = [], [], []
+
+    def follow(kind, n, role=None):
+        then, on = kind[n]
+        if role is not None:
+            on = role if on is None else jnp.logical_and(on, role)
+        when(on, then)
+
+    J, M = joins, middles
+    inner_plan = {1: [(J, 0)], 2: [(J, 1)], 3: [(J, 2)], 4: [(J, 3), (M, 0)], 5: [(J, 4), (J, 5), (M, 1), (M, 2)],
+                  6: [(J, 6), (M, 3), (M, 4)], 7: [(J, 7), (M, 5)], None: [(M, 6), (M, 7)]}
+    end_plan = {1: [(J, 0)], 2: [(J, 1)], 3: [(J, 2), (J, 3), (M, 0)], 6: [(J, 6), (M, 1), (M, 2)],
+                7: [(J, 7), (M, 3)], 8: [(J, 8), (M, 6)], 9: [(J, 9), (M, 7)], None: [(M, 8), (M, 9)]}
 
     def lower(who, on=None):
         cols = span(who * cw, cw)
@@ -654,7 +666,11 @@
         side = remote(part2.at[span((1 - core) * tokens, tokens), cols], xn.at[pl.ds(0, tokens), cols],
                       core2_send.at[who], core2_recv.at[who], (me_f, other_t))
         side_in = landed(xn.at[pl.ds(0, tokens), cols], core2_send.at[who], core2_recv.at[who])
-        plans = [(who % 2 == 0, along_chips(who, cols)), (who % 2 == 1, across_pair(who, cols))]
+        if cw % 256 == 0:
+            cuts = [(None, span(who * cw, cw // 2)), (None, span(who * cw + cw // 2, cw // 2))]
+        else:
+            cuts = [(who % 2 == 0, cols), (who % 2 == 1, cols)]
+        plans = [(cuts[0], along_chips(who, cuts[0][1])), (cuts[1], across_pair(who, cuts[1][1]))]
 
         def run():
             @pl.loop(0, 2)
@@ -666,6 +682,7 @@
                 @pl.when(i == 0)
                 def _():
                     side.start()
+        def join():
             side_in.wait_recv()
 
             @pl.loop(0, tokens // 128)
@@ -673,40 +690,47 @@
                 at = pl.ds(pl.multiple_of(core * tokens + i * 128, 128), 128)
                 more = xn[span(i * 128, 128), cols].astype(F32)
                 part2[at, cols] = (part2[at, cols].astype(F32) + more).astype(BF16)
-            for this, (first, _, _, _) in plans:
+            for (this, _), (first, _, _, _) in plans:
                 def begin():
                     for out, _ in first:
                         out.start()
-                pl.when(this)(begin)
+                when(this, begin)
 
         def middle():
-            for this, (first, second, add, _) in plans:
+            for (this, _), (first, second, add, _) in plans:
                 def pass_on():
                     for _, back in first:
                         back.wait_recv()
                     add()
                     for out, _ in second:
                         out.start()
-                pl.when(this)(pass_on)
+                when(this, pass_on)
 
         def end():
-            for this, (first, second, _, rest) in plans:
+            for (this, cut), (first, second, _, rest) in plans:
                 def close():
                     for _, back in second:
                         back.wait_recv()
-                    total = part2[mine, cols].astype(F32) + rest()
-                    out_ref[:, cols] = (after[:, cols].astype(F32) + total).astype(BF16)
+                    total = part2[mine, cut].astype(F32) + rest()
+                    out_ref[:, cut] = (after[:, cut].astype(F32) + total).astype(BF16)
                     for out, _ in first + second:
                         out.wait_send()
-                pl.when(this)(close)
+                when(this, close)
             side.wait_send()
 
         when(on, run)
+        joins.append((join, on))
         middles.append((middle, on))
         finals.append((end, on))
-        if len(middles) > 2:
-            then, at = middles[-3]
-            when(at, then)
+        n = len(middles) - 1
+        if all_fold:
+            for role, plan in ((inner, inner_plan), (is_end, end_plan)):
+                for kind, k in plan.get(n, ()):
+                    follow(kind, k, role)
+        else:
+            follow(joins, n)
+            if n >= 2:
+                follow(middles, n - 2)
 
     if all_fold:
         inner_order = [[(0, False), (1, False), (0, True), (1, True)],
@@ -780,20 +804,20 @@
                         when(None if all_fold else folds, lambda: tok_wait(mate_sets[part]))
                     for early in range(head):
                         mate_heads(early)
-                    arrivals(inner_order[1])
             if not last:
                 if head == 0:
                     tok_wait(own_set)
                 heads_of(1, head)
         if heads == 1:
             tok_wait(own_set)
+        mate_heads(heads - 1)
+        arrivals(inner_order[1])
         arrivals(inner_order[2])
         line_send_round(0, out=False)
-        mate_heads(heads - 1)
+        heads_of(1, heads - 1)
         arrivals(inner_order[3])
         swaps_in[0].wait_recv()
         line_send_round(1)
-        heads_of(1, heads - 1)
         arrivals(inner_order[4])
 
     def end_front():
@@ -843,16 +867,23 @@
     pl.when(inner)(inner_down)
 
     line_arrive(0, True)
-    line_arrive(1, True)
     for copy, on in xn_sends:
         pl.when(on)(copy.wait_send)
-    mix_end()
-    all_first()
+    for c in range(chunks):
+        mix_chunk(c)
+        if c == 3:
+            line_arrive(1, True)
+        if c > 1:
+            take_pair(c - 2)
     line_arrive(2, False)
     line_arrive(3, False)
     line_arrive(2, True)
-    line_arrive(3, True)
-    all_second()
+    for c in range(chunks - 2, chunks):
+        take_pair(c)
+    for c in range(chunks // 2):
+        if c == chunks // 4:
+            line_arrive(3, True)
+        take_chip(c)
     for k in range(4, per_line):
         line_arrive(k, False)
         line_arrive(k, True)
@@ -863,27 +894,64 @@
         for back in across_in:
             back.wait_recv()
     pl.when(is_end)(end_landed)
-    line_arrive(per_line, True)
     own[2].wait()
     own[3].wait()
-    all_beside()
-    lift(pair)
-    all_third()
+    take_core(to_core)
+    take_core(pair_core)
+    for c in range(chunks // 2, chunks):
+        take_chip(c)
+        take_corner(c - chunks // 2)
+        if c == chunks // 2:
+            lift(chip, pair)
+        elif c == chunks // 2 + 1:
+            lift(chip, 1 - pair)
+    line_arrive(per_line, True)
+    take_core(chip_core)
+    for e in range(1, chips):
+        lift((chip + e) % chips, pair)
+    for c in range(chunks // 2, chunks):
+        take_corner(c)
+    take_core(corner_core)
+    for e in range(1, chips):
+        lift((chip + e) % chips, 1 - pair)
     line_arrive(per_line + 1, True)
-    lift(1 - pair)
-    lower(me_f)
-    lower(other_f)
-    for m in range(per_line, 2 * per_line):
-        if m + 2 < 2 * per_line:
-            line_arrive(m + 2, False)
+    inward = range(1, lines // 2)
+    blocks = [None, None]
+    for dist in range(1, lines):
+        first = per_line + 2 * (dist - 1)
+        for out in (True, False):
+            if out or dist in inward:
+                blocks += [(first, out), (first + 1, out)]
+    for n, this in enumerate(blocks):
+        if this is None:
+            lower(me_f if n == 0 else other_f)
+            continue
+        m, out = this
         _, dist, turn = line_rounds[m]
-        if m >= per_line + 2:
-            line_arrive(m, True)
-        for way in range(2):
-            lower(line_owner(way, dist, turn), line_has(way, dist))
-
-    for then, on in middles[-2:]:
-        when(on, then)
+        if all_fold:
+            if n == 2:
+                pl.when(inner)(lambda: line_arrive(per_line + 2, True))
+            elif n == 5:
+                pl.when(inner)(lambda: line_arrive(per_line + 3, True))
+            if dist == 2:
+                pl.when(is_end)(lambda: line_arrive(m, True))
+            elif dist > 2:
+                line_arrive(m, True)
+        elif dist > 1:
+            line_arrive(m, out)
+        at = line + dist - 2 * dist * upper if out else line - dist + 2 * dist * upper
+        has = jnp.logical_and(at >= 0, at <= lines - 1)
+        if not out:
+            has = jnp.logical_and(has, at // (lines // 2) == upper)
+        lower(2 * at + (pair if turn == 0 else 1 - pair), has)
+
+    if all_fold:
+        for role, plan in ((inner, inner_plan), (is_end, end_plan)):
+            for kind, k in plan[None]:
+                follow(kind, k, role)
+    else:
+        for n in range(len(middles) - 2, len(middles)):
+            follow(middles, n)
     for end, on in finals:
         when(on, end)
     for copy, on in started:
@@ -897,7 +965,7 @@
     in_width = w_query.shape[1] + w_key.shape[1] + w_value.shape[1] + w_gate.shape[1]
     chips = tp // 2
     heads = decay_rate.shape[0]
-    wide = 2 * (1 + 3 * (chips - 1)) + 1
+    wide = CHUNKS * (3 + 4 * (chips - 1))
     vmem = pl.BlockSpec(memory_space=pltpu.VMEM)
     hbm = pl.BlockSpec(memory_space=pl.ANY)
     dma = pltpu.SemaphoreType.DMA
@@ -945,14 +1013,14 @@
             dma((2,)),
             dma((chips,)),
             dma((chips,)),
-            dma((chips - 1,)),
-            dma((chips - 1,)),
+            dma((CHUNKS * (chips - 1),)),
+            dma((CHUNKS * (chips - 1),)),
             dma((wide,)),
             dma((wide,)),
             dma((fs,)),
             dma((fs,)),
-            dma((2 * chips - 1, fs)),
-            dma((2 * chips - 1, fs)),
+            dma((2 * (2 * chips - 1), fs)),
+            dma((2 * (2 * chips - 1), fs)),
         ],
         compiler_params=pltpu.CompilerParams(
             collective_id=0, has_side_effects=True, vmem_limit_bytes=67043328),

time: 232 us -> 206 us (0.89)
  Pallas kernels: 229 us -> 204 us
    pallas_call x1, Pallas kernels: 229 us -> 204 us  [on_device(): pl.pallas_call(functools.partial(kernel, fs, tp), out_shape=jax.ShapeDtyp...]
where the time goes in v2:
time: 206 us
  Pallas kernels  204 us (99%)
  local copies, waits for them, and re-layouts  2.3 us (1%)
    pallas_call x1, Pallas kernels, on_device(): pl.pallas_call(functools.partial(kernel, fs, tp), out_shape=jax.ShapeDtyp...  204 us

profile of v2, /device:TPU:0, one launch (start us, length us, event | category | flops | bytes accessed | tf_op | source)
XLA Modules:
  0.0 205.8 jit_solution(9508032009989609743)
XLA Ops:
  0.0 203.5 %shard_map.109 = bf16[256,2048]{1,0:T(8,128)(2,1)} custom-call(bf16[256,2048]{1,0:T(8,128)(2,1)} %resid_ref.1, f32[1,2048]{1,0:T(1,128)} %bitcast.2, f32[1,2048]{1,0:T(1,128)} %bitcast.3, f32[2]{0:T(128)} %rate_ref.1, bf16[256,256]{1,0:T(8,128)(2,1)} %w1_ref.1, bf16[256,256]{1,0:T(8,128)(2,1)} %w2_ref.1, bf16[256,512]{1,0:T(8,128)(2,1)} %w3_ref.1, ...), custom_call_target="tpu_custom_call" | custom-call | tf_op jit(solution)/shard_map/pallas_call | solution.py:973
  203.5 2.3 %copy.13 = bf16[256,2048]{1,0:T(8,128)(2,1)} copy(bf16[256,2048]{1,0:T(8,128)(2,1)} %shard_map.109) | data formatting | bytes 2097152

commit v3 on v2

--- a/solution.py
+++ b/solution.py
@@ -21,8 +21,8 @@
     return 256 if width % 256 == 0 else 128
 
 
-def kernel(fs, tp, resid_ref, mix_gain_ref, mlp_gain_ref, rate_ref, w1_ref, w2_ref, w3_ref, w4_ref, wo_ref, wu_ref, wd_ref,
-           out_ref, wq, wo, wu, wd, xn, xn2, proj, gated, hidden, part1, core1, chip1, part2, chip2,
+def kernel(fs, tp, resid_hbm, mix_gain_hbm, mlp_gain_hbm, rate_ref, w1_ref, w2_ref, w3_ref, w4_ref, wo_ref, wu_ref, wd_ref,
+           out_ref, resid_ref, mix_gain_ref, mlp_gain_ref, load_sem, out_sem, wq, wo, wu, wd, xn, xn2, proj, gated, hidden, part1, core1, chip1, part2, chip2,
            after, ring_send, ring_recv, own_sem, in_sem, fold_send, fold_recv, put_send, put_recv,
            tok_send, tok_recv, gate_send, gate_recv, aside_send, aside_recv, over_send, over_recv, line_send, line_recv,
            swap_send, swap_recv, core1_send, core1_recv, chip1_send, chip1_recv, all_send, all_recv,
@@ -33,7 +33,7 @@
     in_refs = (w1_ref, w2_ref, w3_ref, w4_ref)
     deep_q = w1_ref.shape[0]
     chips = tp // 2
-    rows = resid_ref.shape[0]
+    rows = resid_hbm.shape[0]
     heads = rate_ref.shape[0]
     tokens = rows * tp
     me_f = lax.axis_index("fs")
@@ -105,6 +105,13 @@
             copy.start()
             loads.append(copy)
             left += w
+
+    row_loads = []
+    for n, (src, dst) in enumerate(((resid_hbm, resid_ref), (mix_gain_hbm, mix_gain_ref),
+                                    (mlp_gain_hbm, mlp_gain_ref))):
+        copy = pltpu.make_async_copy(src, dst, load_sem.at[n])
+        copy.start()
+        row_loads.append(copy)
 
     barrier = pltpu.get_barrier_semaphore()
 
@@ -476,23 +483,30 @@
 
     size = rows // chunks
 
-    def mix_block(x, c):
-        return part1.at[span((2 * x + c) * rows, rows), :]
-
     def mix_out():
         cols = wo.shape[2]
 
-        @pl.loop(0, fs)
-        def _(j):
-            part1[:, span(j * cols, cols)] = jnp.dot(
-                gated[1], wo[j], preferred_element_type=F32).astype(BF16)
         order = [e % chips for e in range(1, chips + 1)]
+        wide_half = part1.shape[1] // 2
+
+        def to_other(e, part):
+            cut = slice(part * wide_half, (part + 1) * wide_half)
+            at = span((2 * ((chip + e) % chips) + 1 - core) * rows, rows)
+            n = 2 * e + part
+            return (part1.at[at, cut], core1.at[e, :, cut], core1_send.at[n], core1_recv.at[n])
+
+        for part in range(2):
+            @pl.loop(0, fs // 2)
+            def _(i):
+                j = i + part * (fs // 2)
+                part1[:, span(j * cols, cols)] = jnp.dot(
+                    gated[1], wo[j], preferred_element_type=F32).astype(BF16)
+            for e in order:
+                go(remote(*to_other(e, part), (me_f, other_t)))
         for e in order:
-            x = (chip + e) % chips
-            go(remote(mix_block(x, 1 - core), core1.at[e], core1_send.at[e], core1_recv.at[e],
-                      (me_f, other_t)))
-        for e in order:
-            landed(core1.at[e], core1_send.at[e], core1_recv.at[e]).wait_recv()
+            for part in range(2):
+                _, dst, s_sem, r_sem = to_other(e, part)
+                landed(dst, s_sem, r_sem).wait_recv()
             if e:
                 for c in range(chunks):
                     at = pl.ds(pl.multiple_of(beside(e) * rows + c * size, size), size)
@@ -578,17 +592,14 @@
             for _, back in (found[c] if isinstance(found[c], list) else [found[c]]):
                 back.wait_recv()
 
-    def lift(x, y=None):
+    def lift(x, y, cores):
         t = tile_of(up_cols)
-        deep_x = 2 * rows if y is None else rows
 
         @pl.loop(0, up_cols // t)
         def _(j):
             cols = span(j * t, t)
-
-            @pl.loop(0, 2)
-            def _(i):
-                at = span(i * tokens + 2 * x * rows + (0 if y is None else y * rows), deep_x)
+            for c in cores:
+                at = span(c * tokens + (2 * x + y) * rows, rows)
                 up = jnp.maximum(jnp.dot(xn2[at, :], wu[:, cols], preferred_element_type=F32), 0.0)
                 hidden[at, cols] = (up * up).astype(BF16)
 
@@ -646,7 +657,7 @@
             return total
         return first, second, add, rest
 
-    finals, joins, middles = [], [], []
+    finals, joins, middles, giving = [], [], [], []
 
     def follow(kind, n, role=None):
         then, on = kind[n]
@@ -670,6 +681,8 @@
             cuts = [(None, span(who * cw, cw // 2)), (None, span(who * cw + cw // 2, cw // 2))]
         else:
             cuts = [(who % 2 == 0, cols), (who % 2 == 1, cols)]
+        given = pltpu.make_async_copy(after.at[:, cols], out_ref.at[:, cols], out_sem.at[who])
+        giving.append((given, on))
         plans = [(cuts[0], along_chips(who, cuts[0][1])), (cuts[1], across_pair(who, cuts[1][1]))]
 
         def run():
@@ -712,10 +725,11 @@
                     for _, back in second:
                         back.wait_recv()
                     total = part2[mine, cut].astype(F32) + rest()
-                    out_ref[:, cut] = (after[:, cut].astype(F32) + total).astype(BF16)
+                    after[:, cut] = (after[:, cut].astype(F32) + total).astype(BF16)
                     for out, _ in first + second:
                         out.wait_send()
                 when(this, close)
+            given.start()
             side.wait_send()
 
         when(on, run)
@@ -759,6 +773,8 @@
             copy.wait()
         send_in(0)
         send_in(1)
+        for copy in row_loads:
+            copy.wait()
         norm_into(xn, tokens + me_t * rows, resid_ref, mix_gain_ref)
         tok_start(own_set)
         for copy in own[1:]:
@@ -828,6 +844,8 @@
         for copy in loads:
             copy.wait()
         puts[0].start()
+        for copy in row_loads:
+            copy.wait()
         norm_into(xn, me_t * rows, resid_ref, mix_gain_ref)
         for out, _ in to_mate:
             out.start()
@@ -902,18 +920,25 @@
         take_chip(c)
         take_corner(c - chunks // 2)
         if c == chunks // 2:
-            lift(chip, pair)
+            lift(chip, pair, (0, 1))
         elif c == chunks // 2 + 1:
-            lift(chip, 1 - pair)
+            lift(chip, 1 - pair, (0, 1))
     line_arrive(per_line, True)
+    others = [(chip + e) % chips for e in range(1, chips)]
+    for x in others:
+        lift(x, pair, (core,))
+    for c in range(chunks // 2, chunks - 2):
+        take_corner(c)
     take_core(chip_core)
-    for e in range(1, chips):
-        lift((chip + e) % chips, pair)
-    for c in range(chunks // 2, chunks):
+    for x in others:
+        lift(x, pair, (1 - core,))
+    for c in range(chunks - 2, chunks):
         take_corner(c)
+    for x in others:
+        lift(x, 1 - pair, (core,))
     take_core(corner_core)
-    for e in range(1, chips):
-        lift((chip + e) % chips, 1 - pair)
+    for x in others:
+        lift(x, 1 - pair, (1 - core,))
     line_arrive(per_line + 1, True)
     inward = range(1, lines // 2)
     blocks = [None, None]
@@ -945,6 +970,11 @@
             has = jnp.logical_and(has, at // (lines // 2) == upper)
         lower(2 * at + (pair if turn == 0 else 1 - pair), has)
 
+    for copy, on in started:
+        when(on, copy.wait_send)
+    early = 2 + 4 * (lines // 2 - 1) if all_fold else 0
+    for end, on in finals[:early]:
+        when(on, end)
     if all_fold:
         for role, plan in ((inner, inner_plan), (is_end, end_plan)):
             for kind, k in plan[None]:
@@ -952,10 +982,10 @@
     else:
         for n in range(len(middles) - 2, len(middles)):
             follow(middles, n)
-    for end, on in finals:
+    for end, on in finals[early:]:
         when(on, end)
-    for copy, on in started:
-        when(on, copy.wait_send)
+    for given, on in giving:
+        when(on, given.wait)
 
 
 def on_device(fs, tp, resid, mix_gain, w_query, w_key, w_value, w_gate, w_output, decay_rate,
@@ -966,16 +996,20 @@
     chips = tp // 2
     heads = decay_rate.shape[0]
     wide = CHUNKS * (3 + 4 * (chips - 1))
-    vmem = pl.BlockSpec(memory_space=pltpu.VMEM)
     hbm = pl.BlockSpec(memory_space=pl.ANY)
     dma = pltpu.SemaphoreType.DMA
     cols = width // fs
     return pl.pallas_call(
         functools.partial(kernel, fs, tp),
         out_shape=jax.ShapeDtypeStruct((rows, width), BF16),
-        in_specs=[vmem] * 3 + [pl.BlockSpec(memory_space=pltpu.SMEM)] + [hbm] * 7,
-        out_specs=vmem,
+        in_specs=[hbm] * 3 + [pl.BlockSpec(memory_space=pltpu.SMEM)] + [hbm] * 7,
+        out_specs=hbm,
         scratch_shapes=[
+            pltpu.VMEM((rows, width), BF16),
+            pltpu.VMEM((1, width), F32),
+            pltpu.VMEM((1, width), F32),
+            dma((3,)),
+            dma((fs,)),
             pltpu.VMEM((heads, width, in_width // heads), BF16),
             pltpu.VMEM((fs, w_output.shape[0], cols), BF16),
             pltpu.VMEM((width, w_up.shape[1] // 2), BF16),
@@ -1011,8 +1045,8 @@
             dma((2, 2 * (fs - 2))),
             dma((2,)),
             dma((2,)),
-            dma((chips,)),
-            dma((chips,)),
+            dma((2 * chips,)),
+            dma((2 * chips,)),
             dma((CHUNKS * (chips - 1),)),
             dma((CHUNKS * (chips - 1),)),
             dma((wide,)),

time: 206 us -> 204 us (level)
  no operation moved by 1% of the time
where the time goes in v3:
time: 204 us
  Pallas kernels  202 us (99%)
  local copies, waits for them, and re-layouts  2.3 us (1%)
    pallas_call x1, Pallas kernels, on_device(): pl.pallas_call(functools.partial(kernel, fs, tp), out_shape=jax.ShapeDtyp...  202 us

profile of v3, /device:TPU:0, one launch (start us, length us, event | category | flops | bytes accessed | tf_op | source)
XLA Modules:
  0.0 204.3 jit_solution(3159570963923991611)
XLA Ops:
  0.0 202.0 %shard_map.109 = bf16[256,2048]{1,0:T(8,128)(2,1)} custom-call(bf16[256,2048]{1,0:T(8,128)(2,1)} %resid_hbm.1, f32[1,2048]{1,0:T(1,128)} %bitcast.2, f32[1,2048]{1,0:T(1,128)} %bitcast.3, f32[2]{0:T(128)} %rate_ref.1, bf16[256,256]{1,0:T(8,128)(2,1)} %w1_ref.1, bf16[256,256]{1,0:T(8,128)(2,1)} %w2_ref.1, bf16[256,512]{1,0:T(8,128)(2,1)} %w3_ref.1, ...), custom_call_target="tpu_custom_call" | custom-call | tf_op jit(solution)/shard_map/pallas_call | solution.py:1002
  202.0 2.3 %copy.13 = bf16[256,2048]{1,0:T(8,128)(2,1)} copy(bf16[256,2048]{1,0:T(8,128)(2,1)} %shard_map.109) | data formatting | bytes 2097152
